TPU v7x, 32 devices: a whole 2x2x4 slice. The times are simulated.
32 devices in a mesh: grp: 2 (over y), sp: 4 (over z), tp: 4 (over x, core).
Axes of the slice: x: 2, y: 2, z: 4, core: 2. Of those that a mesh axis runs over, the one named last changes fastest.
Arguments:
- tokens: bfloat16 [8, 1024, 2048], P('grp', 'sp'), parts along dimension 0, may hold values from -6 to 6
- norm_gain: bfloat16 [2048], replicated, may hold values from 0.099609375 to 1.8984375
- key_weight: bfloat16 [2048, 2048], P(None, 'tp'), may hold values from -0.125 to 0.125
- value_weight: bfloat16 [2048, 2048], P(None, 'tp'), may hold values from -0.125 to 0.125
- break_bias: bfloat16 [8, 1024, 16], P('grp', 'sp', 'tp'), parts along dimension 0, may hold values from -12 to 0
- new_query: bfloat16 [8, 2048], P('grp', 'tp'), parts along dimension 0, may hold values from -6 to 6
Outputs:
- cache_pair: bfloat16 [8, 4, 256, 2, 2048], P(('grp', 'sp'), None, None, None, 'tp'), parts along dimension 0
- cache_bias: bfloat16 [8, 4, 256, 16], P(('grp', 'sp'), None, None, 'tp'), parts along dimension 0
- attended: float32 [8, 2048], P('grp', 'tp'), parts along dimension 0
There are 2 independent parts, one for each index of `grp`. A program takes and returns all parts, laid end to end along the dimension named above; an argument that names none is the same for every part. Nothing has to cross between parts.
All inputs are finite; a program needn't handle non-finite values.
Results may differ from a plain program's by a relative error of at most 0.0064.
Values may be sent and summed in bfloat16 or wider, within the bound.
A program may use at most 64 MiB of HBM per device.

v0:
```python
import jax
import jax.numpy as jnp
from jax import lax
from jax.sharding import PartitionSpec as P

norm_eps = 1e-06


def normalize(tokens, norm_gain):
    widened = tokens.astype(jnp.float32)
    inverse = lax.rsqrt(jnp.mean(widened * widened, axis=-1, keepdims=True) + norm_eps)
    return (widened * inverse * norm_gain.astype(jnp.float32)).astype(jnp.bfloat16)


def project(flat_rows, key_weight, value_weight):
    key_rows = jnp.dot(flat_rows, key_weight, preferred_element_type=jnp.float32).astype(
        jnp.bfloat16
    )
    value_rows = jnp.dot(flat_rows, value_weight, preferred_element_type=jnp.float32).astype(
        jnp.bfloat16
    )
    return (key_rows, value_rows)


def read_placed(new_query, key_rows, value_rows, bias_rows, seq_count):
    block_count, piece, heads_here = bias_rows.shape
    columns = key_rows.shape[2]
    head_size = columns // heads_here
    span = block_count // seq_count
    own_index = lax.axis_index("sp")
    own_seq = own_index // span
    own_part = own_index % span
    own_query = lax.dynamic_slice_in_dim(new_query, own_seq, 1, 0).reshape(heads_here, head_size)
    key_heads = key_rows.reshape(block_count, piece, heads_here, head_size)
    logits = jnp.einsum("hd,nphd->nph", own_query, key_heads, preferred_element_type=jnp.float32)
    logits = logits * head_size ** (-0.5) + bias_rows.astype(jnp.float32)
    keep_log = jax.nn.log_sigmoid(-logits)
    block_totals = jnp.sum(keep_log, axis=1)
    own_slot = (jnp.arange(block_count, dtype=jnp.int32) == own_index)[:, None, None]
    placed = jnp.where(own_slot, block_totals[None], 0.0)
    gathered = lax.psum(placed, "sp")
    same_prompt = lax.dynamic_slice_in_dim(gathered, own_seq * span, span, 0)
    ordered = jnp.transpose(same_prompt, (1, 0, 2)).reshape(block_count * span, heads_here)
    beyond = lax.cumsum(ordered, axis=0, reverse=True) - ordered
    beyond = beyond.reshape(block_count, span, heads_here)
    carried = lax.dynamic_slice_in_dim(beyond, own_part, 1, 1)[:, 0, :]
    later_sum = lax.cumsum(keep_log, axis=1, reverse=True) - keep_log + carried[:, None, :]
    stick_weights = jnp.exp(jax.nn.log_sigmoid(logits) + later_sum).astype(jnp.bfloat16)
    value_heads = value_rows.reshape(block_count, piece, heads_here, head_size)
    mixed = jnp.einsum(
        "nph,nphd->hd", stick_weights, value_heads, preferred_element_type=jnp.float32
    )
    chosen = (jnp.arange(seq_count, dtype=jnp.int32) == own_seq)[:, None]
    partial_rows = jnp.where(chosen, mixed.reshape(1, columns), 0.0)
    return lax.psum(partial_rows, "sp")


def local(tokens, norm_gain, key_weight, value_weight, break_bias, new_query):
    seq_count, tok_rows, width = tokens.shape
    heads_here = break_bias.shape[2]
    block_count = lax.axis_size("sp")
    piece = tok_rows * seq_count // block_count
    columns = key_weight.shape[1]
    normed = normalize(tokens, norm_gain)
    bias_pieces = break_bias.reshape(block_count, piece, heads_here)
    key_rows, value_rows = project(normed.reshape(-1, width), key_weight, value_weight)
    stacked_rows = jnp.stack((key_rows, value_rows), axis=1).reshape(block_count, piece, 2, columns)
    paired, bias_arrived = (
        lax.all_to_all(stacked_rows, "sp", split_axis=0, concat_axis=0, tiled=True),
        lax.all_to_all(bias_pieces, "sp", split_axis=0, concat_axis=0, tiled=True),
    )
    key_rows = paired[:, :, 0]
    value_rows = paired[:, :, 1]
    attended = read_placed(new_query, key_rows, value_rows, bias_arrived, seq_count)
    return (paired[None], bias_arrived[None], attended)


def solution(mesh):
    return jax.shard_map(
        local,
        mesh=mesh,
        in_specs=(
            P("grp", "sp", None),
            P(),
            P(None, "tp"),
            P(None, "tp"),
            P("grp", "sp", "tp"),
            P("grp", "tp"),
        ),
        out_specs=(
            P(("grp", "sp"), None, None, None, "tp"),
            P(("grp", "sp"), None, None, "tp"),
            P("grp", "tp"),
        ),
        check_vma=False,
    )
```

profile of v0, /device:TPU:0, one launch (start us, length us, event | category | flops | bytes accessed | tf_op | source)
XLA Modules:
  0.0 130.2 jit_solution(2703418311215314435)
XLA Ops:
  0.7 6.5 %all-to-all-start.1 = ((bf16[4,256,4]{1,2,0:T(4,128)(2,1)}), bf16[4,256,4]{1,2,0:T(4,128)(2,1)S(1)}, u32[]{:S(2)}, u32[]{:S(2)}) async-start(bf16[4,256,4]{1,2,0:T(4,128)(2,1)} %param.10), calls=%async_computation.1 | async-start | bytes 16384 | tf_op jit(solution)/shard_map/all_to_all | solution.py:70
  7.1 3.2 %fusion = f32[4,256]{1,0:T(4,128)S(1)} fusion(bf16[4,256,2048]{2,1,0:T(8,128)(2,1)} %param.6), kind=kLoop, calls=%fused_computation.2 | loop fusion | flops 6290432 | bytes 4198400 | tf_op jit(solution)/shard_map/reduce_sum | solution.py:11
  10.4 0.2 copy-done.1
  10.6 1.0 fusion.2
  11.6 3.3 %convolution_convert_fusion.1 = bf16[1024,512]{1,0:T(8,128)(2,1)} fusion(bf16[1024,2048]{1,0:T(8,128)(2,1)S(1)} %bitcast.69, bf16[2048,512]{1,0:T(8,128)(2,1)S(1)} %copy-done), kind=kOutput, calls=%fused_computation.7 | convolution fusion | flops 2148007936 | bytes 7340032 | tf_op jit(solution)/shard_map/dot_general | solution.py:16
  15.0 1.5 %copy.18 = bf16[4,256,1,512]{1,3,2,0:T(8,128)(2,1)S(1)} copy(bf16[4,256,1,512]{3,1,0,2:T(8,128)(2,1)} %bitcast.72) | data formatting | bytes 2097152 | tf_op jit(solution)/shard_map/stack | solution.py:67
  16.4 6.2 %convolution_convert_fusion = bf16[1024,512]{1,0:T(8,128)(2,1)} fusion(bf16[1024,2048]{1,0:T(8,128)(2,1)} %bitcast.70, bf16[2048,512]{1,0:T(8,128)(2,1)} %param.9), kind=kOutput, calls=%fused_computation.6 | convolution fusion | flops 2148007936 | bytes 7340032 | tf_op jit(solution)/shard_map/dot_general | solution.py:19
  22.6 2.3 %copy.19 = bf16[4,256,1,512]{1,3,2,0:T(8,128)(2,1)} copy(bf16[4,256,1,512]{3,1,0,2:T(8,128)(2,1)} %bitcast.71) | data formatting | bytes 2097152 | tf_op jit(solution)/shard_map/stack | solution.py:67
  24.9 2.7 %pad_maximum_fusion = bf16[4,256,2,512]{1,3,2,0:T(8,128)(2,1)} fusion(bf16[4,256,1,512]{1,3,2,0:T(8,128)(2,1)} %copy.19, bf16[4,256,1,512]{1,3,2,0:T(8,128)(2,1)S(1)} %copy.18), kind=kLoop, calls=%fused_computation.5 | loop fusion | flops 1048576 | bytes 4194304 | tf_op jit(solution)/shard_map/stack | solution.py:67
  27.6 5.2 %all-to-all-start = ((bf16[4,256,2,512]{1,3,2,0:T(8,128)(2,1)}), bf16[4,256,2,512]{1,3,2,0:T(8,128)(2,1)}, u32[]{:S(2)}, u32[]{:S(2)}) async-start(bf16[4,256,2,512]{1,3,2,0:T(8,128)(2,1)} %pad_maximum_fusion), calls=%async_computation | async-start | bytes 4194304 | tf_op jit(solution)/shard_map/all_to_all | solution.py:69
  32.8 47.8 %all-to-all-done = bf16[4,256,2,512]{1,3,2,0:T(8,128)(2,1)} async-done(((bf16[4,256,2,512]{1,3,2,0:T(8,128)(2,1)}), bf16[4,256,2,512]{1,3,2,0:T(8,128)(2,1)}, u32[]{:S(2)}, u32[]{:S(2)}) %all-to-all-start) | async-done | bytes 2097184 | tf_op jit(solution)/shard_map/all_to_all | solution.py:69
  80.6 1.7 %fusion.20 = (bf16[4,256,1,512]{1,3,2,0:T(8,128)(2,1)S(1)}, bf16[4,256,1,512]{1,3,2,0:T(8,128)(2,1)S(1)}) fusion(bf16[4,256,2,512]{1,3,2,0:T(8,128)(2,1)} %all-to-all-done), kind=kLoop, calls=%fused_computation.37 | loop fusion | bytes 4194304 | tf_op jit(solution)/shard_map/slice | solution.py:72
  82.3 0.2 fusion.5
  82.5 0.1 negate_bitcast_fusion
  82.7 10.0 %psum.14 = f32[4,4,4]{2,1,0:T(4,128)S(1)} all-reduce(f32[4,4,4]{2,1,0:T(4,128)S(1)} %broadcast_select_fusion.1), channel_id=1, replica_groups=mesh['grp'=2,'sp'=4,'tp'=4] {'sp'}, use_global_device_ids=true, to_apply=%region_4.5 | all-reduce | flops 64 | bytes 512 | tf_op jit(solution)/shard_map/psum | solution.py:41
  92.8 20.1 %reduce-window.6 = f32[4,4,2,128]{3,2,1,0:T(2,128)S(1)} reduce-window(f32[4,4,2,128]{3,2,1,0:T(2,128)S(1)} %reshape.54, f32[]{:T(128)} %constant.36.clone.1), window={size=1x1x1x128 pad=0_0x0_0x0_0x0_127}, to_apply=%region_1.2 | reduce-window | flops 520192 | bytes 32772 | tf_op jit(solution)/shard_map/reduce-window
  112.9 0.1 copy.21
  113.1 0.1 copy.22
  113.2 0.1 broadcast_add_fusion
  113.3 0.1 fusion.13
  113.4 0.4 fusion.3
  113.8 9.6 %psum.15 = f32[4,512]{1,0:T(4,128)} all-reduce(f32[4,512]{1,0:T(4,128)S(1)} %broadcast_select_fusion), channel_id=1, replica_groups=mesh['grp'=2,'sp'=4,'tp'=4] {'sp'}, use_global_device_ids=true, to_apply=%region_6.7 | all-reduce | flops 2048 | bytes 16384 | tf_op jit(solution)/shard_map/psum | solution.py:55
  123.5 6.2 %copy.24 = bf16[1,4,256,2,512]{4,3,2,1,0:T(2,128)(2,1)} copy(bf16[1,4,256,2,512]{2,4,3,1,0:T(8,128)(2,1)} %bitcast.3) | data formatting | bytes 4194304
  129.6 0.6 copy.51
  (23 shorter events, 0.3 us)
Async XLA Ops:
  0.6 11.0 %copy-start = (bf16[2048,512]{1,0:T(8,128)(2,1)S(1)}, bf16[2048,512]{1,0:T(8,128)(2,1)}, u32[]{:S(2)}) copy-start(bf16[2048,512]{1,0:T(8,128)(2,1)} %param.8) | copy-start | bytes 6291460
  0.6 9.7 %copy-start.3 = (bf16[2048]{0:T(1024)(128)(2,1)S(1)}, bf16[2048]{0:T(1024)(128)(2,1)}, u32[]{:S(2)}) copy-start(bf16[2048]{0:T(1024)(128)(2,1)} %param.7) | copy-start | bytes 12292
  0.7 27.0 %all-to-all-start.1 = ((bf16[4,256,4]{1,2,0:T(4,128)(2,1)}), bf16[4,256,4]{1,2,0:T(4,128)(2,1)S(1)}, u32[]{:S(2)}, u32[]{:S(2)}) async-start(bf16[4,256,4]{1,2,0:T(4,128)(2,1)} %param.10), calls=%async_computation.1 | async-start | bytes 16384 | tf_op jit(solution)/shard_map/all_to_all | solution.py:70
  7.1 3.4 %copy-start.1 = (bf16[4,256,2048]{2,1,0:T(8,128)(2,1)S(1)}, bf16[4,256,2048]{2,1,0:T(8,128)(2,1)}, u32[]{:S(2)}) copy-start(bf16[4,256,2048]{2,1,0:T(8,128)(2,1)} %param.6) | copy-start | bytes 12582916
  11.6 3.3 %copy-start.2 = (bf16[4,256,2048]{2,1,0:T(8,128)(2,1)}, bf16[4,256,2048]{2,1,0:T(8,128)(2,1)S(1)}, u32[]{:S(2)}) copy-start(bf16[4,256,2048]{2,1,0:T(8,128)(2,1)S(1)} %fusion.2) | copy-start | bytes 12582916
  27.6 54.7 %copy-start.4 = (bf16[4,512]{1,0:T(4,128)(2,1)S(1)}, bf16[4,512]{1,0:T(4,128)(2,1)}, u32[]{:S(2)}) copy-start(bf16[4,512]{1,0:T(4,128)(2,1)} %param.11) | copy-start | bytes 12292
  27.6 53.0 %all-to-all-start = ((bf16[4,256,2,512]{1,3,2,0:T(8,128)(2,1)}), bf16[4,256,2,512]{1,3,2,0:T(8,128)(2,1)}, u32[]{:S(2)}, u32[]{:S(2)}) async-start(bf16[4,256,2,512]{1,3,2,0:T(8,128)(2,1)} %pad_maximum_fusion), calls=%async_computation | async-start | bytes 4194304 | tf_op jit(solution)/shard_map/all_to_all | solution.py:69
where the time goes:
time: 131 us; the launch traced here: 130 us
  waiting for transfers between devices  47.8 us (36%)
  other arithmetic  27.6 us (21%)
  blocking collectives  19.6 us (15%)
  local copies, waits for them, and re-layouts  12.7 us (10%)
  starting transfers between devices  11.7 us (9%)
  matrix products  10.1 us (8%)
    all_to_all x1, waiting for transfers between devices, local(): lax.all_to_all(stacked_rows, 'sp', split_axis=0, concat_axis=0, tiled=True)  47.8 us
    another operation x2, other arithmetic  20.1 us
    psum x1, blocking collectives, read_placed(): gathered = lax.psum(placed, 'sp')  9.95 us
    psum x1, blocking collectives, read_placed(): return lax.psum(partial_rows, 'sp')  9.64 us
    unnamed x12, local copies, waits for them, and re-layouts  6.96 us
    all_to_all x1, starting transfers between devices, local(): lax.all_to_all(bias_pieces, 'sp', split_axis=0, concat_axis=0, tiled=True)  6.49 us
    dot_general x1, matrix products, project(): jnp.dot(flat_rows, value_weight, preferred_element_type=jnp.float32)  6.16 us
    all_to_all x1, starting transfers between devices, local(): lax.all_to_all(stacked_rows, 'sp', split_axis=0, concat_axis=0, tiled=True)  5.22 us
  transfers between devices with their start and end apart: 2, of which 1 were waited for; matrix products, arithmetic and copies ran while one was open for 16% of the time, Pallas kernels for 0%

commit v1 on v0

--- a/solution.py
+++ b/solution.py
@@ -1,6 +1,10 @@
+import functools
+
 import jax
 import jax.numpy as jnp
 from jax import lax
+from jax.experimental import pallas as pl
+from jax.experimental.pallas import tpu as pltpu
 from jax.sharding import PartitionSpec as P
 
 norm_eps = 1e-06
@@ -75,9 +79,300 @@
     return (paired[None], bias_arrived[None], attended)
 
 
+MESH = pl.DeviceIdType.MESH
+CHUNKS = 4
+
+
+def partner_table(n):
+    return [sorted((k for k in range(n) if k != c), key=lambda k: (abs(k - c), k)) for c in range(n)]
+
+
+def pick(table, step, me):
+    chosen = jnp.int32(table[0][step])
+    for c in range(1, len(table)):
+        chosen = jnp.where(me == c, jnp.int32(table[c][step]), chosen)
+    return chosen
+
+
+def gather_kernel(
+    n,
+    tok_ref,
+    gain_ref,
+    wk_ref,
+    wv_ref,
+    bias_ref,
+    query_ref,
+    pair_ref,
+    bias_out,
+    att_out,
+    tok,
+    nrm,
+    wk,
+    wv,
+    keys,
+    vals,
+    lsc,
+    wsc,
+    attbuf,
+    z_send,
+    z_recv,
+    x_send,
+    x_recv,
+    d_send,
+    d_recv,
+    e_send,
+    e_recv,
+    b_send,
+    b_recv,
+    a_send,
+    a_recv,
+    own_sem,
+    w_sem,
+):
+    me = lax.axis_index("sp")
+    t = lax.axis_index("tp")
+    tp = lax.axis_size("tp")
+    piece, width = tok.shape[1:]
+    columns = wk.shape[1]
+    heads = bias_ref.shape[1]
+    head_size = columns // heads
+    quarter = piece // tp
+    rows = quarter // CHUNKS
+    mate = t + 1 - 2 * lax.rem(t, 2)
+    cross = lax.rem(t + 2, tp)
+    table = partner_table(n)
+    partners = [pick(table, j, me) for j in range(n - 1)]
+
+    barrier = pltpu.get_barrier_semaphore()
+    for p in partners:
+        pl.semaphore_signal(barrier, inc=1, device_id={"sp": p}, device_id_type=MESH)
+    pl.semaphore_signal(barrier, inc=1, device_id={"tp": mate}, device_id_type=MESH)
+    pl.semaphore_signal(barrier, inc=1, device_id={"tp": cross}, device_id_type=MESH)
+
+    own_copy = pltpu.make_async_copy(tok_ref.at[me], tok.at[me], own_sem)
+    own_copy.start()
+    wk_copy = pltpu.make_async_copy(wk_ref, wk, w_sem.at[0])
+    wk_copy.start()
+    wv_copy = pltpu.make_async_copy(wv_ref, wv, w_sem.at[1])
+    wv_copy.start()
+    pl.semaphore_wait(barrier, n + 1)
+
+    def span_of(owner, q):
+        return pl.ds(pl.multiple_of(owner * quarter + q * rows, rows), rows)
+
+    def hop(src, dst, send, recv, where):
+        return pltpu.make_async_remote_copy(
+            src_ref=src, dst_ref=dst, send_sem=send, recv_sem=recv, device_id=where, device_id_type=MESH
+        )
+
+    def z_copy(p, source, q):
+        at = span_of(t, q)
+        return hop(
+            tok_ref.at[p, at], tok.at[source, at], z_send.at[p, q], z_recv.at[source, q], {"sp": p}
+        )
+
+    def share(block, owner, q, send, recv, to):
+        at = span_of(owner, q)
+        return hop(
+            tok.at[block, at], tok.at[block, at], send.at[block, q], recv.at[block, q], {"tp": to}
+        )
+
+    def bias_copy(p, source):
+        return hop(bias_ref.at[p], bias_out.at[source], b_send.at[p], b_recv.at[source], {"sp": p})
+
+    def att_copy(p, source):
+        return hop(attbuf.at[source], attbuf.at[source], a_send.at[p], a_recv.at[source], {"sp": p})
+
+    for p in partners:
+        for q in range(CHUNKS):
+            z_copy(p, me, q).start()
+    for p in partners:
+        bias_copy(p, me).start()
+    bias_out[me] = bias_ref[me]
+
+    row_at = lax.broadcasted_iota(jnp.int32, (8, columns), 0)
+    head_at = lax.broadcasted_iota(jnp.int32, (8, columns), 1) // head_size
+    seq_at = lax.broadcasted_iota(jnp.int32, query_ref.shape, 0)
+    own_query = jnp.sum(
+        jnp.where(seq_at == me, query_ref[...].astype(jnp.float32), 0.0), axis=0, keepdims=True
+    )
+    spread = jnp.where(row_at == head_at, own_query, 0.0).astype(jnp.bfloat16)
+    gain = gain_ref[...].astype(jnp.float32)
+    groups = piece // 128
+    tile = 128
+    out_row = lax.broadcasted_iota(jnp.int32, (2 * tile, 2 * tile), 0)
+    in_row = lax.broadcasted_iota(jnp.int32, (2 * tile, 2 * tile), 1)
+    zip_rows = jnp.where(in_row == out_row // 2 + lax.rem(out_row, 2) * tile, 1.0, 0.0).astype(
+        jnp.bfloat16
+    )
+
+    def key_part(block):
+        step_rows = 16
+
+        def norm_rows(i, carry):
+            at = pl.ds(pl.multiple_of(i * step_rows, step_rows), step_rows)
+            widened = tok[block, at, :].astype(jnp.float32)
+            inverse = lax.rsqrt(jnp.mean(widened * widened, axis=-1, keepdims=True) + norm_eps)
+            nrm[at, :] = (widened * inverse * gain).astype(jnp.bfloat16)
+            return carry
+
+        lax.fori_loop(0, piece // step_rows, norm_rows, 0, unroll=2)
+        key_rows = jnp.dot(nrm[...], wk[...], preferred_element_type=jnp.float32).astype(jnp.bfloat16)
+        keys[...] = key_rows
+        logits = lax.dot_general(
+            spread, key_rows, (((1,), (1,)), ((), ())), preferred_element_type=jnp.float32
+        ) * head_size ** (-0.5)
+        for g in range(groups):
+            lsc[block * groups + g] = logits[:, g * 128 : (g + 1) * 128]
+
+    def value_part(block):
+        value_rows = jnp.dot(nrm[...], wv[...], preferred_element_type=jnp.float32).astype(
+            jnp.bfloat16
+        )
+        vals[block] = value_rows
+        for i in range(piece // tile):
+            both = jnp.concatenate(
+                [keys[i * tile : (i + 1) * tile, :], value_rows[i * tile : (i + 1) * tile, :]], axis=0
+            )
+            zipped = jnp.dot(zip_rows, both, preferred_element_type=jnp.float32).astype(jnp.bfloat16)
+            pair_ref[block, i * tile : (i + 1) * tile] = zipped.reshape(tile, 2, columns)
+
+    previous = me
+    own_copy.wait()
+    for j in range(n - 1):
+        block = partners[j]
+        for q in range(CHUNKS):
+            z_copy(block, block, q).wait_recv()
+            share(block, t, q, x_send, x_recv, cross).start()
+            share(block, t, q, d_send, d_recv, mate).start()
+            if q == 0:
+                if j == 0:
+                    wk_copy.wait()
+                key_part(previous)
+            if q == 1:
+                if j == 0:
+                    wv_copy.wait()
+                value_part(previous)
+            if q >= 1:
+                share(block, cross, q - 1, x_send, x_recv, cross).wait_recv()
+                share(block, cross, q - 1, e_send, e_recv, mate).start()
+        share(block, cross, CHUNKS - 1, x_send, x_recv, cross).wait_recv()
+        share(block, cross, CHUNKS - 1, e_send, e_recv, mate).start()
+        for q in range(CHUNKS):
+            share(block, mate, q, d_send, d_recv, mate).wait_recv()
+            share(block, mate, q, e_send, e_recv, mate).wait_recv()
+        previous = block
+    key_part(previous)
+    value_part(previous)
+
+    for p in partners:
+        bias_copy(p, p).wait_recv()
+    after = jnp.where(
+        lax.broadcasted_iota(jnp.int32, (128, 128), 0) > lax.broadcasted_iota(jnp.int32, (128, 128), 1),
+        1.0,
+        0.0,
+    )
+    carried = jnp.zeros((8, 1), jnp.float32)
+    for g in range(n * groups - 1, -1, -1):
+        lanes = slice((g % groups) * 128, (g % groups + 1) * 128)
+        lsc[g, 0:heads] = lsc[g, 0:heads] + bias_out[g // groups, :, lanes].astype(jnp.float32)
+        logits = lsc[g]
+        soft = jnp.log1p(jnp.exp(-jnp.abs(logits)))
+        take_log = jnp.minimum(logits, 0.0) - soft
+        keep_log = jnp.minimum(-logits, 0.0) - soft
+        later = (
+            jnp.dot(
+                keep_log, after, precision=lax.Precision.HIGHEST, preferred_element_type=jnp.float32
+            )
+            + carried
+        )
+        wsc[:, g * 128 : (g + 1) * 128] = jnp.exp(take_log + later).astype(jnp.bfloat16)
+        carried = carried + jnp.sum(keep_log, axis=1, keepdims=True)
+    mixed = jnp.dot(
+        wsc[...], vals[...].reshape(n * piece, columns), preferred_element_type=jnp.float32
+    )
+    attbuf[me] = jnp.sum(jnp.where(row_at == head_at, mixed, 0.0), axis=0, keepdims=True)
+    for p in partners:
+        att_copy(p, me).start()
+    for p in partners:
+        for q in range(CHUNKS):
+            z_copy(p, me, q).wait_send()
+            share(p, t, q, x_send, x_recv, cross).wait_send()
+            share(p, t, q, d_send, d_recv, mate).wait_send()
+            share(p, cross, q, e_send, e_recv, mate).wait_send()
+        bias_copy(p, me).wait_send()
+    for p in partners:
+        att_copy(p, p).wait_recv()
+    for s in range(n):
+        att_out[s : s + 1, :] = attbuf[s]
+    for p in partners:
+        att_copy(p, me).wait_send()
+
+
+def fused(tokens, norm_gain, key_weight, value_weight, break_bias, new_query):
+    n, piece, width = tokens.shape
+    heads = break_bias.shape[2]
+    columns = key_weight.shape[1]
+    bias = jnp.transpose(break_bias, (0, 2, 1))
+    vmem = pl.BlockSpec(memory_space=pltpu.VMEM)
+    anywhere = pl.BlockSpec(memory_space=pl.ANY)
+    dma = pltpu.SemaphoreType.DMA
+    pair, bias_placed, attended = pl.pallas_call(
+        functools.partial(gather_kernel, n),
+        out_shape=(
+            jax.ShapeDtypeStruct((n, piece, 2, columns), jnp.bfloat16),
+            jax.ShapeDtypeStruct((n, heads, piece), jnp.bfloat16),
+            jax.ShapeDtypeStruct((n, columns), jnp.float32),
+        ),
+        in_specs=[anywhere, vmem, anywhere, anywhere, vmem, vmem],
+        out_specs=(vmem, vmem, vmem),
+        scratch_shapes=[
+            pltpu.VMEM((n, piece, width), jnp.bfloat16),
+            pltpu.VMEM((piece, width), jnp.bfloat16),
+            pltpu.VMEM(key_weight.shape, jnp.bfloat16),
+            pltpu.VMEM(value_weight.shape, jnp.bfloat16),
+            pltpu.VMEM((piece, columns), jnp.bfloat16),
+            pltpu.VMEM((n, piece, columns), jnp.bfloat16),
+            pltpu.VMEM((n * piece // 128, 8, 128), jnp.float32),
+            pltpu.VMEM((8, n * piece), jnp.bfloat16),
+            pltpu.VMEM((n, 1, columns), jnp.float32),
+        ]
+        + [dma((n, CHUNKS))] * 8
+        + [dma((n,))] * 4
+        + [dma, dma((2,))],
+        compiler_params=pltpu.CompilerParams(
+            collective_id=0, has_side_effects=True, vmem_limit_bytes=48 * 1024 * 1024
+        ),
+        name="gather_read",
+    )(tokens, norm_gain.reshape(1, width), key_weight, value_weight, bias, new_query)
+    return (pair[None], jnp.transpose(bias_placed, (0, 2, 1))[None], attended)
+
+
+def suits(mesh, tokens, break_bias, key_weight):
+    n, tp = mesh.shape["sp"], mesh.shape["tp"]
+    seq_count, tok_rows, width = tokens.shape
+    heads, columns = break_bias.shape[2], key_weight.shape[1]
+    return (
+        seq_count == n
+        and tp == 4
+        and n > 1
+        and tok_rows % (tp * CHUNKS * 16) == 0
+        and tok_rows % 128 == 0
+        and heads <= 8
+        and columns % heads == 0
+        and (columns // heads) % 128 == 0
+        and width % 128 == 0
+    )
+
+
 def solution(mesh):
+    def step(tokens, norm_gain, key_weight, value_weight, break_bias, new_query):
+        if suits(mesh, tokens, break_bias, key_weight):
+            return fused(tokens, norm_gain, key_weight, value_weight, break_bias, new_query)
+        return local(tokens, norm_gain, key_weight, value_weight, break_bias, new_query)
+
     return jax.shard_map(
-        local,
+        step,
         mesh=mesh,
         in_specs=(
             P("grp", "sp", None),

time: 131 us -> 62.1 us (0.47)
  Pallas kernels: 0 us -> 55 us
  waiting for transfers between devices: 47.8 us -> 0 us
  other arithmetic: 27.6 us -> 0 us
  blocking collectives: 19.6 us -> 0 us
  starting transfers between devices: 11.7 us -> 0 us
  matrix products: 10.1 us -> 0 us
  local copies, waits for them, and re-layouts: 12.7 us -> 6.18 us
    pallas_call x0 -> x1, Pallas kernels: none -> 55 us  [fused(): pl.pallas_call(functools.partial(gather_kernel, n), out_shape=(jax.ShapeD...]
    all_to_all x2 -> x0, waiting for transfers between devices: 47.8 us -> none  [the longest x1 47.8 us: local(): lax.all_to_all(stacked_rows, 'sp', split_axis=0, concat_axis=0, tiled=True)]
    another operation x5 -> x0, other arithmetic: 23 us -> none
    psum x2 -> x0, blocking collectives: 19.6 us -> none  [the longest x1 9.95 us: read_placed(): gathered = lax.psum(placed, 'sp')]
    all_to_all x2 -> x0, starting transfers between devices: 11.7 us -> none  [the longest x1 6.49 us: local(): lax.all_to_all(bias_pieces, 'sp', split_axis=0, concat_axis=0, tiled=True)]
    dot_general x4 -> x0, matrix products: 10.1 us -> none  [the longest x1 6.16 us: project(): jnp.dot(flat_rows, value_weight, preferred_element_type=jnp.float32)]
    another operation x6 -> x0, local copies, waits for them, and re-layouts: 3.9 us -> none  [the longest x2 3.75 us: local(): jnp.stack((key_rows, value_rows), axis=1)]
    reduce_sum x1 -> x0, other arithmetic: 3.23 us -> none  [normalize(): jnp.mean(widened * widened, axis=-1, keepdims=True) + norm_eps]
  transfers between devices with their start and end apart: 2 -> 0, of which waited for: 1 -> 0; matrix products, arithmetic and copies ran while one was open for 16% -> 0% of each run, Pallas kernels for 0% -> 0%
where the time goes in v1:
time: 62.1 us; the launch traced here: 61.8 us
  Pallas kernels  55 us (89%)
  local copies, waits for them, and re-layouts  6.18 us (10%)
  between operations  0.64 us (1%)
    pallas_call x1, Pallas kernels, fused(): pl.pallas_call(functools.partial(gather_kernel, n), out_shape=(jax.ShapeD...  55 us
    unnamed x9, local copies, waits for them, and re-layouts  5.49 us

profile of v1, /device:TPU:0, one launch (start us, length us, event | category | flops | bytes accessed | tf_op | source)
XLA Modules:
  0.0 61.8 jit_solution(9440281892632738225)
XLA Ops:
  0.6 0.7 %reshape.9.gain_ref = bf16[1,2048]{1,0:T(2,128)(2,1)S(1)} reshape(bf16[2048]{0:T(1024)(128)(2,1)} %param.7) | data formatting | bytes 8192 | tf_op jit(solution)/shard_map/reshape | solution.py:347
  1.3 0.0 copy-start
  1.3 1.6 %copy-done = bf16[2048,512]{1,0:T(8,128)(2,1)S(1)} copy-done((bf16[2048,512]{1,0:T(8,128)(2,1)S(1)}, bf16[2048,512]{1,0:T(8,128)(2,1)}, u32[]{:S(2)}) %copy-start) | copy-done | bytes 2097176
  2.9 0.0 copy-start.1
  2.9 0.7 %copy-done.1 = bf16[4,256,4]{1,2,0:T(4,128)(2,1)S(1)} copy-done((bf16[4,256,4]{1,2,0:T(4,128)(2,1)S(1)}, bf16[4,256,4]{1,2,0:T(4,128)(2,1)}, u32[]{:S(2)}) %copy-start.1) | copy-done | bytes 8216
  3.6 0.0 copy-start.2
  3.6 0.7 %copy-done.2 = bf16[4,512]{1,0:T(4,128)(2,1)S(1)} copy-done((bf16[4,512]{1,0:T(4,128)(2,1)S(1)}, bf16[4,512]{1,0:T(4,128)(2,1)}, u32[]{:S(2)}) %copy-start.2) | copy-done | bytes 4120
  4.3 55.0 %gather_read.1 = (bf16[4,256,2,512]{3,2,1,0:T(2,128)(2,1)S(1)}, bf16[4,4,256]{2,1,0:T(4,128)(2,1)S(1)}, f32[4,512]{1,0:T(4,128)S(1)}) custom-call(bf16[4,256,2048]{2,1,0:T(8,128)(2,1)} %tok_ref.1, bf16[1,2048]{1,0:T(2,128)(2,1)S(1)} %reshape.9.gain_ref, bf16[2048,512]{1,0:T(8,128)(2,1)S(1)} %copy-done, bf16[2048,512]{1,0:T(8,128)(2,1)} %wv_ref.1, ...), custom_call_target="tpu_custom_call" | custom-call | tf_op jit(solution)/shard_map/gather_read/pallas_call | solution.py:320
  59.3 1.3 %copy.12 = bf16[1,4,256,2,512]{4,3,2,1,0:T(2,128)(2,1)} copy(bf16[1,4,256,2,512]{4,3,2,1,0:T(2,128)(2,1)S(1)} %bitcast.5) | data formatting | bytes 4194304
  60.6 0.6 copy.13
  61.2 0.6 copy.14
Async XLA Ops:
  1.3 1.6 %copy-start = (bf16[2048,512]{1,0:T(8,128)(2,1)S(1)}, bf16[2048,512]{1,0:T(8,128)(2,1)}, u32[]{:S(2)}) copy-start(bf16[2048,512]{1,0:T(8,128)(2,1)} %wk_ref.1) | copy-start | bytes 6291460
  2.9 0.7 %copy-start.1 = (bf16[4,256,4]{1,2,0:T(4,128)(2,1)S(1)}, bf16[4,256,4]{1,2,0:T(4,128)(2,1)}, u32[]{:S(2)}) copy-start(bf16[4,256,4]{1,2,0:T(4,128)(2,1)} %param.10) | copy-start | bytes 24580
  3.6 0.7 %copy-start.2 = (bf16[4,512]{1,0:T(4,128)(2,1)S(1)}, bf16[4,512]{1,0:T(4,128)(2,1)}, u32[]{:S(2)}) copy-start(bf16[4,512]{1,0:T(4,128)(2,1)} %query_ref.1) | copy-start | bytes 12292

commit v2 on v1

--- a/solution.py
+++ b/solution.py
@@ -84,13 +84,31 @@
 
 
 def partner_table(n):
-    return [sorted((k for k in range(n) if k != c), key=lambda k: (abs(k - c), k)) for c in range(n)]
-
-
-def pick(table, step, me):
-    chosen = jnp.int32(table[0][step])
+    return [
+        [(p,) for p in sorted(set(range(n)) - {c}, key=lambda p: (abs(p - c) > 1, -abs(p - c), p))]
+        for c in range(n)
+    ]
+
+
+def send_table(n):
+    def rank(c, p):
+        span = abs(p - c)
+        return (n - 1 - c if p < c else c) > (c if p < c else n - 1 - c), span > 1, -span, p
+
+    return [
+        [
+            (p, q)
+            for p in sorted(set(range(n)) - {c}, key=lambda p: rank(c, p))
+            for q in range(CHUNKS)
+        ]
+        for c in range(n)
+    ]
+
+
+def pick(table, step, part, me):
+    chosen = jnp.int32(table[0][step][part])
     for c in range(1, len(table)):
-        chosen = jnp.where(me == c, jnp.int32(table[c][step]), chosen)
+        chosen = jnp.where(me == c, jnp.int32(table[c][step][part]), chosen)
     return chosen
 
 
@@ -114,6 +132,8 @@
     lsc,
     wsc,
     attbuf,
+    query,
+    gains,
     z_send,
     z_recv,
     x_send,
@@ -128,6 +148,7 @@
     a_recv,
     own_sem,
     w_sem,
+    s_sem,
 ):
     me = lax.axis_index("sp")
     t = lax.axis_index("tp")
@@ -136,16 +157,21 @@
     columns = wk.shape[1]
     heads = bias_ref.shape[1]
     head_size = columns // heads
-    quarter = piece // tp
-    rows = quarter // CHUNKS
+    half = piece // (tp // 2)
+    rows = half // CHUNKS
+    side = t // 2
+    core = lax.rem(t, 2)
+    other = (tp // 2 - 1) - side
     mate = t + 1 - 2 * lax.rem(t, 2)
     cross = lax.rem(t + 2, tp)
     table = partner_table(n)
-    partners = [pick(table, j, me) for j in range(n - 1)]
+    partners = [pick(table, j, 0, me) for j in range(n - 1)]
+    order = send_table(n)
 
     barrier = pltpu.get_barrier_semaphore()
     for p in partners:
         pl.semaphore_signal(barrier, inc=1, device_id={"sp": p}, device_id_type=MESH)
+        pl.semaphore_signal(barrier, inc=1, device_id={"sp": p, "tp": mate}, device_id_type=MESH)
     pl.semaphore_signal(barrier, inc=1, device_id={"tp": mate}, device_id_type=MESH)
     pl.semaphore_signal(barrier, inc=1, device_id={"tp": cross}, device_id_type=MESH)
 
@@ -155,10 +181,17 @@
     wk_copy.start()
     wv_copy = pltpu.make_async_copy(wv_ref, wv, w_sem.at[1])
     wv_copy.start()
-    pl.semaphore_wait(barrier, n + 1)
+    small = [
+        pltpu.make_async_copy(bias_ref.at[me], bias_out.at[me], s_sem.at[0]),
+        pltpu.make_async_copy(query_ref, query, s_sem.at[1]),
+        pltpu.make_async_copy(gain_ref, gains, s_sem.at[2]),
+    ]
+    for copy in small:
+        copy.start()
+    pl.semaphore_wait(barrier, 2 * n)
 
     def span_of(owner, q):
-        return pl.ds(pl.multiple_of(owner * quarter + q * rows, rows), rows)
+        return pl.ds(pl.multiple_of(owner * half + q * rows, rows), rows)
 
     def hop(src, dst, send, recv, where):
         return pltpu.make_async_remote_copy(
@@ -166,9 +199,13 @@
         )
 
     def z_copy(p, source, q):
-        at = span_of(t, q)
+        at = span_of(side, q)
         return hop(
-            tok_ref.at[p, at], tok.at[source, at], z_send.at[p, q], z_recv.at[source, q], {"sp": p}
+            tok_ref.at[p, at],
+            tok.at[source, at],
+            z_send.at[p, q],
+            z_recv.at[source, q],
+            {"sp": p, "tp": mate},
         )
 
     def share(block, owner, q, send, recv, to):
@@ -184,20 +221,25 @@
         return hop(attbuf.at[source], attbuf.at[source], a_send.at[p], a_recv.at[source], {"sp": p})
 
     for p in partners:
-        for q in range(CHUNKS):
+        bias_copy(p, me).start()
+
+    @pl.when(core == 0)
+    def send_tokens():
+        for k in range((n - 1) * CHUNKS):
+            p, q = pick(order, k, 0, me), pick(order, k, 1, me)
             z_copy(p, me, q).start()
-    for p in partners:
-        bias_copy(p, me).start()
-    bias_out[me] = bias_ref[me]
+
+    for copy in small:
+        copy.wait()
 
     row_at = lax.broadcasted_iota(jnp.int32, (8, columns), 0)
     head_at = lax.broadcasted_iota(jnp.int32, (8, columns), 1) // head_size
-    seq_at = lax.broadcasted_iota(jnp.int32, query_ref.shape, 0)
+    seq_at = lax.broadcasted_iota(jnp.int32, query.shape, 0)
     own_query = jnp.sum(
-        jnp.where(seq_at == me, query_ref[...].astype(jnp.float32), 0.0), axis=0, keepdims=True
+        jnp.where(seq_at == me, query[...].astype(jnp.float32), 0.0), axis=0, keepdims=True
     )
     spread = jnp.where(row_at == head_at, own_query, 0.0).astype(jnp.bfloat16)
-    gain = gain_ref[...].astype(jnp.float32)
+    gain = gains[...].astype(jnp.float32).reshape(1, width)
     groups = piece // 128
     tile = 128
     out_row = lax.broadcasted_iota(jnp.int32, (2 * tile, 2 * tile), 0)
@@ -239,28 +281,37 @@
 
     previous = me
     own_copy.wait()
+    def relay(block, start, stop):
+        @pl.when(core == 1)
+        def relay_chunks():
+            for q in range(start, stop):
+                if q < CHUNKS:
+                    z_copy(block, block, q).wait_recv()
+                    share(block, side, q, x_send, x_recv, cross).start()
+                    share(block, side, q, d_send, d_recv, mate).start()
+                if q >= 1:
+                    share(block, other, q - 1, x_send, x_recv, cross).wait_recv()
+                    share(block, other, q - 1, e_send, e_recv, mate).start()
+
+    def arrive(block):
+        @pl.when(core == 0)
+        def wait_chunks():
+            for q in range(CHUNKS):
+                share(block, side, q, d_send, d_recv, mate).wait_recv()
+                share(block, other, q, e_send, e_recv, mate).wait_recv()
+
     for j in range(n - 1):
         block = partners[j]
-        for q in range(CHUNKS):
-            z_copy(block, block, q).wait_recv()
-            share(block, t, q, x_send, x_recv, cross).start()
-            share(block, t, q, d_send, d_recv, mate).start()
-            if q == 0:
-                if j == 0:
-                    wk_copy.wait()
-                key_part(previous)
-            if q == 1:
-                if j == 0:
-                    wv_copy.wait()
-                value_part(previous)
-            if q >= 1:
-                share(block, cross, q - 1, x_send, x_recv, cross).wait_recv()
-                share(block, cross, q - 1, e_send, e_recv, mate).start()
-        share(block, cross, CHUNKS - 1, x_send, x_recv, cross).wait_recv()
-        share(block, cross, CHUNKS - 1, e_send, e_recv, mate).start()
-        for q in range(CHUNKS):
-            share(block, mate, q, d_send, d_recv, mate).wait_recv()
-            share(block, mate, q, e_send, e_recv, mate).wait_recv()
+        relay(block, 0, 2)
+        if j == 0:
+            wk_copy.wait()
+        key_part(previous)
+        relay(block, 2, 3)
+        if j == 0:
+            wv_copy.wait()
+        value_part(previous)
+        relay(block, 3, CHUNKS + 1)
+        arrive(block)
         previous = block
     key_part(previous)
     value_part(previous)
@@ -295,12 +346,22 @@
     for p in partners:
         att_copy(p, me).start()
     for p in partners:
-        for q in range(CHUNKS):
-            z_copy(p, me, q).wait_send()
-            share(p, t, q, x_send, x_recv, cross).wait_send()
-            share(p, t, q, d_send, d_recv, mate).wait_send()
-            share(p, cross, q, e_send, e_recv, mate).wait_send()
         bias_copy(p, me).wait_send()
+
+    @pl.when(core == 0)
+    def sent_tokens():
+        for p in partners:
+            for q in range(CHUNKS):
+                z_copy(p, me, q).wait_send()
+
+    @pl.when(core == 1)
+    def sent_shares():
+        for p in partners:
+            for q in range(CHUNKS):
+                share(p, side, q, x_send, x_recv, cross).wait_send()
+                share(p, side, q, d_send, d_recv, mate).wait_send()
+                share(p, other, q, e_send, e_recv, mate).wait_send()
+
     for p in partners:
         att_copy(p, p).wait_recv()
     for s in range(n):
@@ -315,7 +376,7 @@
     columns = key_weight.shape[1]
     bias = jnp.transpose(break_bias, (0, 2, 1))
     vmem = pl.BlockSpec(memory_space=pltpu.VMEM)
-    anywhere = pl.BlockSpec(memory_space=pl.ANY)
+    hbm = pl.BlockSpec(memory_space=pltpu.HBM)
     dma = pltpu.SemaphoreType.DMA
     pair, bias_placed, attended = pl.pallas_call(
         functools.partial(gather_kernel, n),
@@ -324,7 +385,7 @@
             jax.ShapeDtypeStruct((n, heads, piece), jnp.bfloat16),
             jax.ShapeDtypeStruct((n, columns), jnp.float32),
         ),
-        in_specs=[anywhere, vmem, anywhere, anywhere, vmem, vmem],
+        in_specs=[hbm] * 6,
         out_specs=(vmem, vmem, vmem),
         scratch_shapes=[
             pltpu.VMEM((n, piece, width), jnp.bfloat16),
@@ -336,15 +397,17 @@
             pltpu.VMEM((n * piece // 128, 8, 128), jnp.float32),
             pltpu.VMEM((8, n * piece), jnp.bfloat16),
             pltpu.VMEM((n, 1, columns), jnp.float32),
+            pltpu.VMEM(new_query.shape, jnp.bfloat16),
+            pltpu.VMEM((width,), jnp.bfloat16),
         ]
         + [dma((n, CHUNKS))] * 8
         + [dma((n,))] * 4
-        + [dma, dma((2,))],
+        + [dma, dma((2,)), dma((3,))],
         compiler_params=pltpu.CompilerParams(
             collective_id=0, has_side_effects=True, vmem_limit_bytes=48 * 1024 * 1024
         ),
         name="gather_read",
-    )(tokens, norm_gain.reshape(1, width), key_weight, value_weight, bias, new_query)
+    )(tokens, norm_gain, key_weight, value_weight, bias, new_query)
     return (pair[None], jnp.transpose(bias_placed, (0, 2, 1))[None], attended)
 
 
@@ -356,7 +419,7 @@
         seq_count == n
         and tp == 4
         and n > 1
-        and tok_rows % (tp * CHUNKS * 16) == 0
+        and tok_rows % (tp // 2 * CHUNKS * 16) == 0
         and tok_rows % 128 == 0
         and heads <= 8
         and columns % heads == 0

time: 62.1 us -> 53.3 us (0.86)
  Pallas kernels: 55 us -> 46.2 us
    pallas_call x1, Pallas kernels: 55 us -> 46.2 us  [fused(): pl.pallas_call(functools.partial(gather_kernel, n), out_shape=(jax.ShapeD...]
    reshape x1 -> x0, local copies, waits for them, and re-layouts: 0.69 us -> none  [fused(): norm_gain.reshape(1, width)]
    unnamed x9 -> x11, local copies, waits for them, and re-layouts: 5.49 us -> 6.17 us
where the time goes in v2:
time: 53.3 us; the launch traced here: 53.1 us
  Pallas kernels  46.2 us (87%)
  local copies, waits for them, and re-layouts  6.17 us (12%)
  between operations  0.65 us (1%)
    pallas_call x1, Pallas kernels, fused(): pl.pallas_call(functools.partial(gather_kernel, n), out_shape=(jax.ShapeD...  46.2 us
    unnamed x11, local copies, waits for them, and re-layouts  6.17 us

profile of v2, /device:TPU:0, one launch (start us, length us, event | category | flops | bytes accessed | tf_op | source)
XLA Modules:
  0.0 53.1 jit_solution(15655976793080518980)
XLA Ops:
  0.6 0.0 copy-start
  0.6 1.6 %copy-done = bf16[2048,512]{1,0:T(8,128)(2,1)S(1)} copy-done((bf16[2048,512]{1,0:T(8,128)(2,1)S(1)}, bf16[2048,512]{1,0:T(8,128)(2,1)}, u32[]{:S(2)}) %copy-start) | copy-done | bytes 2097176
  2.2 0.0 copy-start.1
  2.2 0.7 %copy-done.1 = bf16[4,256,4]{1,2,0:T(4,128)(2,1)S(1)} copy-done((bf16[4,256,4]{1,2,0:T(4,128)(2,1)S(1)}, bf16[4,256,4]{1,2,0:T(4,128)(2,1)}, u32[]{:S(2)}) %copy-start.1) | copy-done | bytes 8216
  2.9 0.0 copy-start.2
  2.9 0.7 %copy-done.2 = bf16[2048]{0:T(1024)(128)(2,1)S(1)} copy-done((bf16[2048]{0:T(1024)(128)(2,1)S(1)}, bf16[2048]{0:T(1024)(128)(2,1)}, u32[]{:S(2)}) %copy-start.2) | copy-done | bytes 4120
  3.6 0.0 copy-start.3
  3.6 0.7 %copy-done.3 = bf16[4,512]{1,0:T(4,128)(2,1)S(1)} copy-done((bf16[4,512]{1,0:T(4,128)(2,1)S(1)}, bf16[4,512]{1,0:T(4,128)(2,1)}, u32[]{:S(2)}) %copy-start.3) | copy-done | bytes 4120
  4.3 46.2 %gather_read.1 = (bf16[4,256,2,512]{3,2,1,0:T(2,128)(2,1)S(1)}, bf16[4,4,256]{2,1,0:T(4,128)(2,1)S(1)}, f32[4,512]{1,0:T(4,128)S(1)}) custom-call(bf16[4,256,2048]{2,1,0:T(8,128)(2,1)} %tok_ref.1, bf16[2048]{0:T(1024)(128)(2,1)S(1)} %copy-done.2, bf16[2048,512]{1,0:T(8,128)(2,1)S(1)} %copy-done, bf16[2048,512]{1,0:T(8,128)(2,1)} %wv_ref.1, ...), custom_call_target="tpu_custom_call" | custom-call | tf_op jit(solution)/shard_map/gather_read/pallas_call | solution.py:381
  50.5 1.3 %copy.12 = bf16[1,4,256,2,512]{4,3,2,1,0:T(2,128)(2,1)} copy(bf16[1,4,256,2,512]{4,3,2,1,0:T(2,128)(2,1)S(1)} %bitcast.5) | data formatting | bytes 4194304
  51.9 0.6 %copy.13 = bf16[1,4,256,4]{2,3,1,0:T(4,128)(2,1)} copy(bf16[1,4,256,4]{2,3,1,0:T(4,128)(2,1)S(1)} %bitcast.6) | data formatting | bytes 16384
  52.5 0.6 %copy.14 = f32[4,512]{1,0:T(4,128)} copy(f32[4,512]{1,0:T(4,128)S(1)} %get-tuple-element.14) | data formatting | bytes 16384
Async XLA Ops:
  0.6 1.6 %copy-start = (bf16[2048,512]{1,0:T(8,128)(2,1)S(1)}, bf16[2048,512]{1,0:T(8,128)(2,1)}, u32[]{:S(2)}) copy-start(bf16[2048,512]{1,0:T(8,128)(2,1)} %wk_ref.1) | copy-start | bytes 6291460
  2.2 0.7 %copy-start.1 = (bf16[4,256,4]{1,2,0:T(4,128)(2,1)S(1)}, bf16[4,256,4]{1,2,0:T(4,128)(2,1)}, u32[]{:S(2)}) copy-start(bf16[4,256,4]{1,2,0:T(4,128)(2,1)} %param.10) | copy-start | bytes 24580
  2.9 0.7 %copy-start.2 = (bf16[2048]{0:T(1024)(128)(2,1)S(1)}, bf16[2048]{0:T(1024)(128)(2,1)}, u32[]{:S(2)}) copy-start(bf16[2048]{0:T(1024)(128)(2,1)} %gain_ref.1) | copy-start | bytes 12292
  3.6 0.7 %copy-start.3 = (bf16[4,512]{1,0:T(4,128)(2,1)S(1)}, bf16[4,512]{1,0:T(4,128)(2,1)}, u32[]{:S(2)}) copy-start(bf16[4,512]{1,0:T(4,128)(2,1)} %query_ref.1) | copy-start | bytes 12292

commit v3 on v2

--- a/solution.py
+++ b/solution.py
@@ -302,15 +302,15 @@
 
     for j in range(n - 1):
         block = partners[j]
-        relay(block, 0, 2)
+        relay(block, 0, 1)
         if j == 0:
             wk_copy.wait()
         key_part(previous)
-        relay(block, 2, 3)
+        relay(block, 1, 2)
         if j == 0:
             wv_copy.wait()
         value_part(previous)
-        relay(block, 3, CHUNKS + 1)
+        relay(block, 2, CHUNKS + 1)
         arrive(block)
         previous = block
     key_part(previous)

time: 53.3 us -> 50.9 us (0.955)
  Pallas kernels: 46.2 us -> 43.8 us
    pallas_call x1, Pallas kernels: 46.2 us -> 43.8 us  [fused(): pl.pallas_call(functools.partial(gather_kernel, n), out_shape=(jax.ShapeD...]
where the time goes in v3:
time: 50.9 us; the launch traced here: 50.6 us
  Pallas kernels  43.8 us (86%)
  local copies, waits for them, and re-layouts  6.17 us (12%)
  between operations  0.65 us (1%)
    pallas_call x1, Pallas kernels, fused(): pl.pallas_call(functools.partial(gather_kernel, n), out_shape=(jax.ShapeD...  43.8 us
    unnamed x11, local copies, waits for them, and re-layouts  6.17 us

profile of v3, /device:TPU:0, one launch (start us, length us, event | category | flops | bytes accessed | tf_op | source)
XLA Modules:
  0.0 50.6 jit_solution(2877657480264113403)
XLA Ops:
  0.6 0.0 copy-start
  0.6 1.6 %copy-done = bf16[2048,512]{1,0:T(8,128)(2,1)S(1)} copy-done((bf16[2048,512]{1,0:T(8,128)(2,1)S(1)}, bf16[2048,512]{1,0:T(8,128)(2,1)}, u32[]{:S(2)}) %copy-start) | copy-done | bytes 2097176
  2.2 0.0 copy-start.1
  2.2 0.7 %copy-done.1 = bf16[4,256,4]{1,2,0:T(4,128)(2,1)S(1)} copy-done((bf16[4,256,4]{1,2,0:T(4,128)(2,1)S(1)}, bf16[4,256,4]{1,2,0:T(4,128)(2,1)}, u32[]{:S(2)}) %copy-start.1) | copy-done | bytes 8216
  2.9 0.0 copy-start.2
  2.9 0.7 %copy-done.2 = bf16[2048]{0:T(1024)(128)(2,1)S(1)} copy-done((bf16[2048]{0:T(1024)(128)(2,1)S(1)}, bf16[2048]{0:T(1024)(128)(2,1)}, u32[]{:S(2)}) %copy-start.2) | copy-done | bytes 4120
  3.6 0.0 copy-start.3
  3.6 0.7 %copy-done.3 = bf16[4,512]{1,0:T(4,128)(2,1)S(1)} copy-done((bf16[4,512]{1,0:T(4,128)(2,1)S(1)}, bf16[4,512]{1,0:T(4,128)(2,1)}, u32[]{:S(2)}) %copy-start.3) | copy-done | bytes 4120
  4.3 43.8 %gather_read.1 = (bf16[4,256,2,512]{3,2,1,0:T(2,128)(2,1)S(1)}, bf16[4,4,256]{2,1,0:T(4,128)(2,1)S(1)}, f32[4,512]{1,0:T(4,128)S(1)}) custom-call(bf16[4,256,2048]{2,1,0:T(8,128)(2,1)} %tok_ref.1, bf16[2048]{0:T(1024)(128)(2,1)S(1)} %copy-done.2, bf16[2048,512]{1,0:T(8,128)(2,1)S(1)} %copy-done, bf16[2048,512]{1,0:T(8,128)(2,1)} %wv_ref.1, ...), custom_call_target="tpu_custom_call" | custom-call | tf_op jit(solution)/shard_map/gather_read/pallas_call | solution.py:381
  48.1 1.3 %copy.12 = bf16[1,4,256,2,512]{4,3,2,1,0:T(2,128)(2,1)} copy(bf16[1,4,256,2,512]{4,3,2,1,0:T(2,128)(2,1)S(1)} %bitcast.5) | data formatting | bytes 4194304
  49.4 0.6 %copy.13 = bf16[1,4,256,4]{2,3,1,0:T(4,128)(2,1)} copy(bf16[1,4,256,4]{2,3,1,0:T(4,128)(2,1)S(1)} %bitcast.6) | data formatting | bytes 16384
  50.0 0.6 %copy.14 = f32[4,512]{1,0:T(4,128)} copy(f32[4,512]{1,0:T(4,128)S(1)} %get-tuple-element.14) | data formatting | bytes 16384
Async XLA Ops:
  0.6 1.6 %copy-start = (bf16[2048,512]{1,0:T(8,128)(2,1)S(1)}, bf16[2048,512]{1,0:T(8,128)(2,1)}, u32[]{:S(2)}) copy-start(bf16[2048,512]{1,0:T(8,128)(2,1)} %wk_ref.1) | copy-start | bytes 6291460
  2.2 0.7 %copy-start.1 = (bf16[4,256,4]{1,2,0:T(4,128)(2,1)S(1)}, bf16[4,256,4]{1,2,0:T(4,128)(2,1)}, u32[]{:S(2)}) copy-start(bf16[4,256,4]{1,2,0:T(4,128)(2,1)} %param.10) | copy-start | bytes 24580
  2.9 0.7 %copy-start.2 = (bf16[2048]{0:T(1024)(128)(2,1)S(1)}, bf16[2048]{0:T(1024)(128)(2,1)}, u32[]{:S(2)}) copy-start(bf16[2048]{0:T(1024)(128)(2,1)} %gain_ref.1) | copy-start | bytes 12292
  3.6 0.7 %copy-start.3 = (bf16[4,512]{1,0:T(4,128)(2,1)S(1)}, bf16[4,512]{1,0:T(4,128)(2,1)}, u32[]{:S(2)}) copy-start(bf16[4,512]{1,0:T(4,128)(2,1)} %query_ref.1) | copy-start | bytes 12292
